TPU v7x, 32 devices: a whole 2x2x4 slice. The times are simulated.
32 devices in a mesh: grp: 2 (over y), fs: 8 (over z, core), tp: 2 (over x).
Axes of the slice: x: 2, y: 2, z: 4, core: 2. Of those that a mesh axis runs over, the one named last changes fastest.
Arguments:
- prompt: bfloat16 [6144, 2048], P(('grp', 'fs')), parts along dimension 0, may hold values from -6 to 6
- routes: int32 [6144, 4], P(('grp', 'fs')), parts along dimension 0, may hold values from 0 to 7, all different within a row; in each aligned block of 384 rows (0 to 383, 384 to 767, ...) at most 240 rows name the same one
- route_weight: float32 [6144, 4], P(('grp', 'fs')), parts along dimension 0, may hold values from 0.2 to 1
- norm_gain: float32 [2048], P('fs'), may hold values from 0.1 to 1.9
- gate_train: float32 [8, 2048, 1024], P(None, 'fs', 'tp'), may hold values from -0.4 to 0.4
- up_train: float32 [8, 2048, 1024], P(None, 'fs', 'tp'), may hold values from -0.4 to 0.4
- down_train: float32 [8, 1024, 2048], P(None, 'fs', 'tp'), may hold values from -0.07 to 0.07
Outputs:
- gate_serve: bfloat16 [16, 2048, 1024], P(('grp', 'fs'), None, 'tp'), parts along dimension 0
- up_serve: bfloat16 [16, 2048, 1024], P(('grp', 'fs'), None, 'tp'), parts along dimension 0
- down_serve: bfloat16 [16, 1024, 2048], P(('grp', 'fs'), 'tp'), parts along dimension 0
- mixed: bfloat16 [6144, 2048], P(('grp', 'fs'), 'tp'), parts along dimension 0
There are 2 independent parts, one for each index of `grp`. A program takes and returns all parts, laid end to end along the dimension named above; an argument that names none is the same for every part. Nothing has to cross between parts.
Inputs may be any that keep to these rules, and one draw needn't show every extreme that they name: `routes`: each row names 4 different experts. Among the rows of one index of fs no expert is named more than 240 times, a bound that some block reaches on some index.
All inputs are finite; a program needn't handle non-finite values.
Results may differ from a plain program's by a relative error of at most 0.012.
Values may be sent and summed in bfloat16 or wider, within the bound.
A program may use at most 128 MiB of HBM per device.

v0:
```python
import jax
import jax.numpy as jnp
from jax import lax
from jax.sharding import PartitionSpec as P

TOP = 4


LIMIT = 7.0
ALPHA = 1.702
EPS = 1e-06


def shards(prompt, routes, route_weight, norm_gain, gate_train, up_train, down_train):
    gate_cast = (norm_gain[None, :, None] * gate_train).astype(jnp.bfloat16)
    up_cast = (norm_gain[None, :, None] * up_train).astype(jnp.bfloat16)
    down_cast = down_train.astype(jnp.bfloat16)
    gate_mine, up_mine = (
        lax.all_to_all(gate_cast, "fs", split_axis=0, concat_axis=1, tiled=True),
        lax.all_to_all(up_cast, "fs", split_axis=0, concat_axis=1, tiled=True),
    )
    down_rows = lax.all_to_all(down_cast, "fs", split_axis=0, concat_axis=1, tiled=True)
    down_mine = lax.all_to_all(down_rows, "tp", split_axis=1, concat_axis=2, tiled=True)
    tok_rows, width = prompt.shape
    experts = gate_train.shape[0]
    quarter = width // lax.axis_size("tp")
    capacity = min(tok_rows, max(2, 5 * tok_rows * TOP // (4 * experts)))
    values = prompt.astype(jnp.float32)
    normed = (values * lax.rsqrt(jnp.mean(values * values, axis=-1, keepdims=True) + EPS)).astype(
        jnp.bfloat16
    )
    flat_expert = routes.reshape(-1)
    onehot = (flat_expert[:, None] == jnp.arange(experts, dtype=jnp.int32)[None, :]).astype(
        jnp.int32
    )
    earlier = jnp.cumsum(onehot, axis=0) - onehot
    slot_pos = jnp.sum(earlier * onehot, axis=1)
    target = flat_expert * capacity + slot_pos
    source_row = jnp.arange(tok_rows * TOP, dtype=jnp.int32) // TOP
    outbox = jnp.zeros((experts * capacity, width), jnp.bfloat16).at[target].set(normed[source_row])
    inbox = lax.all_to_all(
        outbox.reshape(experts, capacity, width), "fs", split_axis=0, concat_axis=1, tiled=True
    )
    gate_pre = jnp.einsum("erd,edf->erf", inbox, gate_mine, preferred_element_type=jnp.float32)
    up_pre = jnp.einsum("erd,edf->erf", inbox, up_mine, preferred_element_type=jnp.float32)
    gate_pre = jnp.minimum(gate_pre, LIMIT)
    up_pre = jnp.clip(up_pre, -LIMIT, LIMIT)
    hidden = ((up_pre + 1.0) * gate_pre * jax.nn.sigmoid(ALPHA * gate_pre)).astype(jnp.bfloat16)
    own_width = hidden.shape[2]
    empty = jnp.zeros((hidden.shape[0], hidden.shape[1], down_rows.shape[2]), jnp.float32)
    total = empty
    piece = lax.all_gather(hidden, "tp", axis=2, tiled=True)
    for index in range(piece.shape[2] // own_width):
        cols = piece[:, :, index * own_width : (index + 1) * own_width]
        weight_rows = lax.dynamic_slice_in_dim(down_rows, index * own_width, own_width, 1)
        part = jnp.einsum(
            "erf,efd->erd", cols, weight_rows, preferred_element_type=jnp.float32
        ).astype(jnp.bfloat16)
        total = total + part.astype(jnp.float32)
    summed = total.astype(jnp.bfloat16)
    back = lax.all_to_all(summed, "fs", split_axis=1, concat_axis=0, tiled=True)
    picked = back.reshape(experts * capacity, quarter)[target].astype(jnp.float32)
    weighted = picked.reshape(tok_rows, TOP, quarter) * route_weight[:, :, None]
    mixed = jnp.sum(weighted, axis=1).astype(jnp.bfloat16)
    return (gate_mine, up_mine, down_mine, mixed)


def solution(mesh):
    return jax.shard_map(
        shards,
        mesh=mesh,
        in_specs=(
            P(("grp", "fs"), None),
            P(("grp", "fs"), None),
            P(("grp", "fs"), None),
            P("fs"),
            P(None, "fs", "tp"),
            P(None, "fs", "tp"),
            P(None, "fs", "tp"),
        ),
        out_specs=(
            P(("grp", "fs"), None, "tp"),
            P(("grp", "fs"), None, "tp"),
            P(("grp", "fs"), "tp", None),
            P(("grp", "fs"), "tp"),
        ),
        check_vma=False,
    )
```

profile of v0, /device:TPU:0, one launch (start us, length us, event | category | flops | bytes accessed | tf_op | source)
XLA Modules:
  0.0 601.1 jit_solution(9907944391653193153)
XLA Ops:
  7.2 6.8 %multiply_convert_fusion = (bf16[8,256,512]{2,1,0:T(8,128)(2,1)}, bf16[8,256,512]{2,1,0:T(8,128)(2,1)}) fusion(f32[8,256,512]{2,1,0:T(8,128)} %param.12, f32[256]{0:T(256)} %param.10, f32[8,256,512]{2,1,0:T(8,128)} %param.11), kind=kLoop, calls=%fused_computation.7 | loop fusion | flops 4194304 | bytes 12583936 | tf_op jit(solution)/shard_map/convert_element_type | solution.py:16
  14.0 6.5 %all-to-all-start = ((bf16[8,256,512]{2,1,0:T(8,128)(2,1)}), bf16[8,256,512]{2,1,0:T(8,128)(2,1)S(1)}, u32[]{:S(2)}, u32[]{:S(2)}) async-start(bf16[8,256,512]{2,1,0:T(8,128)(2,1)} %get-tuple-element.17), calls=%async_computation | async-start | bytes 4194304 | tf_op jit(solution)/shard_map/all_to_all | solution.py:19
  20.5 0.1 copy.32
  20.6 0.1 eq.29
  20.8 0.1 eq.25
  20.9 2.3 reduce-window.6
  23.2 0.3 slice_reduce_fusion
  23.5 0.2 reduce-window.9
  23.7 0.1 copy.31
  23.8 0.2 mul.72
  24.0 0.3 fusion.12
  24.3 0.1 add_bitcast_fusion
  24.5 1.8 fusion.4
  26.3 2.9 fusion.5
  29.2 33.3 %scatter_custom_fusion = bf16[1920,2048]{1,0:T(8,128)(2,1)} fusion(s32[1536]{0:T(1024)S(1)} %fusion.11, bf16[384,2048]{1,0:T(8,128)(2,1)} %fusion.5, s32[2048]{0:T(1024)S(1)} %pad_clamp_fusion.1, bf16[]{:T(256)} %constant.17.clone.1), kind=kCustom, calls=%fused_computation.4 | custom fusion | bytes 7864832 | tf_op jit(solution)/shard_map/scatter | solution.py:40
  62.5 7.0 %all-to-all-done = bf16[8,256,512]{2,1,0:T(8,128)(2,1)S(1)} async-done(((bf16[8,256,512]{2,1,0:T(8,128)(2,1)}), bf16[8,256,512]{2,1,0:T(8,128)(2,1)S(1)}, u32[]{:S(2)}, u32[]{:S(2)}) %all-to-all-start) | async-done | bytes 2097184 | tf_op jit(solution)/shard_map/all_to_all | solution.py:19
  69.5 178.2 %all_to_all.72 = bf16[8,240,2048]{2,1,0:T(8,128)(2,1)} all-to-all(bf16[8,240,2048]{2,1,0:T(8,128)(2,1)} %bitcast.61), channel_id=1, replica_groups=mesh['grp'=2,'fs'=8,'tp'=2] {'fs'}, dimensions={0} | all-to-all | bytes 15728640 | tf_op jit(solution)/shard_map/all_to_all | solution.py:41
  247.7 4.4 all-to-all-start.1
  252.1 9.5 %fusion.13 = f32[1920,512]{1,0:T(8,128)} fusion(bf16[1920,2048]{1,0:T(8,128)(2,1)} %bitcast.73, bf16[2048,512]{1,0:T(8,128)(2,1)S(1)} %bitcast.70), kind=kOutput, calls=%fused_computation.45 | convolution fusion | flops 4026531840 | bytes 13893632 | tf_op jit(solution)/shard_map/erd,edf->erf/dot_general | solution.py:44
  261.6 39.5 %all-to-all-done.1 = bf16[8,256,512]{2,1,0:T(8,128)(2,1)} async-done(((bf16[8,256,512]{2,1,0:T(8,128)(2,1)}), bf16[8,256,512]{2,1,0:T(8,128)(2,1)}, u32[]{:S(2)}, u32[]{:S(2)}) %all-to-all-start.1) | async-done | bytes 2097184 | tf_op jit(solution)/shard_map/all_to_all | solution.py:20
  301.1 11.8 %multiply_convert_fusion.2 = bf16[1920,512]{1,0:T(8,128)(2,1)} fusion(f32[1920,512]{1,0:T(8,128)} %fusion.13, bf16[1920,2048]{1,0:T(8,128)(2,1)} %bitcast.74, bf16[2048,512]{1,0:T(8,128)(2,1)} %bitcast.8), kind=kOutput, calls=%fused_computation.11 | convolution fusion | flops 4036362240 | bytes 15859712 | tf_op jit(solution)/shard_map/erd,edf->erf/dot_general | solution.py:45
  312.9 2.5 convert_element_type.62
  315.4 51.6 %all_to_all.73 = bf16[8,128,1024]{2,1,0:T(8,128)(2,1)S(1)} all-to-all(bf16[8,128,1024]{2,1,0:T(8,128)(2,1)S(1)} %convert_element_type.62), channel_id=1, replica_groups=mesh['grp'=2,'fs'=8,'tp'=2] {'fs'}, dimensions={0} | all-to-all | bytes 4194304 | tf_op jit(solution)/shard_map/all_to_all | solution.py:22
  367.1 1.3 copy-done
  368.4 5.2 copy.46
  373.5 0.5 broadcast.146
  374.1 12.8 %reduce.6 = bf16[1024,1024]{1,0:T(8,128)(2,1)S(1)} reduce(bf16[1024,1,1024]{2,1,0:T(2,128)(2,1)} %bitcast.64, bf16[]{:T(256)} %broadcast.146), dimensions={1}, to_apply=%bitcast.58.reduce_sub_computation | reduce | bytes 4194306
  386.8 2.5 reshape.227
  389.4 4.0 all-to-all-start.3
  393.4 4.2 fusion.6
  397.6 2.3 fusion.2
  399.9 27.0 %copy.45 = bf16[1,1920,1024]{2,0,1:T(2,128)(2,1)} copy(bf16[1,1920,1024]{2,1,0:T(8,128)(2,1)S(1)} %fusion.2) | data formatting | bytes 7864320 | tf_op jit(solution)/shard_map/convert_element_type | solution.py:60
  426.8 24.6 %reduce.7 = bf16[1920,1024]{1,0:T(8,128)(2,1)} reduce(bf16[1920,1,1024]{2,1,0:T(2,128)(2,1)} %bitcast.62, bf16[]{:T(256)} %broadcast.146), dimensions={1}, to_apply=%bitcast.57.reduce_sub_computation | reduce | bytes 7864322
  451.4 7.6 %reshape.225 = bf16[8,2,122880]{2,1,0:T(2,128)(2,1)} reshape(bf16[1920,1024]{1,0:T(8,128)(2,1)} %reduce.7) | data formatting | bytes 7864320
  459.1 4.9 all-to-all-start.5
  464.0 0.1 copy.35
  464.2 3.1 reshape.228
  467.3 3.0 copy.37
  470.3 2.6 copy.30
  472.8 3.9 copy.36
  476.7 75.6 %all-to-all-done.5 = bf16[8,2,122880]{2,1,0:T(2,128)(2,1)} async-done(((bf16[8,2,122880]{2,1,0:T(2,128)(2,1)}), bf16[8,2,122880]{2,1,0:T(2,128)(2,1)}, u32[]{:S(2)}, u32[]{:S(2)}) %all-to-all-start.5) | async-done | bytes 3932192 | tf_op jit(solution)/shard_map/all_to_all | solution.py:61
  552.4 8.5 %reshape.226 = bf16[1920,1,1024]{2,1,0:T(2,128)(2,1)} reshape(bf16[8,2,122880]{2,1,0:T(2,128)(2,1)} %all-to-all-done.5) | data formatting | bytes 7864320
  560.8 6.8 %copy.44 = bf16[1,1920,1024]{2,1,0:T(8,128)(2,1)} copy(bf16[1,1920,1024]{2,0,1:T(2,128)(2,1)} %bitcast.63) | data formatting | bytes 7864320
  567.7 9.7 %gather_fusion = bf16[1536,1024]{1,0:T(8,128)(2,1)S(1)} fusion(bf16[1920,1024]{1,0:T(8,128)(2,1)} %bitcast.60, s32[2048]{0:T(1024)S(1)} %pad_clamp_fusion), kind=kCustom, calls=%fused_computation.1 | custom fusion | bytes 6297600 | tf_op jit(solution)/shard_map/gather | solution.py:62
  577.4 4.4 reshape.190
  581.8 7.9 %multiply_reduce_fusion = bf16[384,1024]{1,0:T(8,128)(2,1)} fusion(f32[384,4,1024]{2,1,0:T(4,128)} %reshape.190, f32[384,4]{1,0:T(8,128)S(1)} %copy.35), kind=kLoop, calls=%fused_computation.6 | loop fusion | flops 2752512 | bytes 7084032 | tf_op jit(solution)/shard_map/reduce_sum | solution.py:64
  589.6 1.3 copy.49
  591.0 3.0 copy.50
  (24 shorter events, 0.2 us)
Async XLA Ops:
  14.0 6.5 %copy-start.4 = (s32[384,4]{0,1:T(4,128)S(1)}, s32[384,4]{0,1:T(4,128)}, u32[]{:S(2)}) copy-start(s32[384,4]{0,1:T(4,128)} %param.8) | copy-start | bytes 18436
  14.0 55.5 %all-to-all-start = ((bf16[8,256,512]{2,1,0:T(8,128)(2,1)}), bf16[8,256,512]{2,1,0:T(8,128)(2,1)S(1)}, u32[]{:S(2)}, u32[]{:S(2)}) async-start(bf16[8,256,512]{2,1,0:T(8,128)(2,1)} %get-tuple-element.17), calls=%async_computation | async-start | bytes 4194304 | tf_op jit(solution)/shard_map/all_to_all | solution.py:19
  69.5 182.6 %copy-start.2 = (bf16[8,256,512]{2,1,0:T(8,128)(2,1)}, bf16[8,256,512]{2,1,0:T(8,128)(2,1)S(1)}, u32[]{:S(2)}) copy-start(bf16[8,256,512]{2,1,0:T(8,128)(2,1)S(1)} %all-to-all-done) | copy-start | bytes 6291460
  247.7 53.4 %all-to-all-start.1 = ((bf16[8,256,512]{2,1,0:T(8,128)(2,1)}), bf16[8,256,512]{2,1,0:T(8,128)(2,1)}, u32[]{:S(2)}, u32[]{:S(2)}) async-start(bf16[8,256,512]{2,1,0:T(8,128)(2,1)} %get-tuple-element.16), calls=%async_computation.1 | async-start | bytes 4194304 | tf_op jit(solution)/shard_map/all_to_all | solution.py:20
  252.1 141.3 %all-gather.3.cloned.1.call-start = ((), (), s32[]{:S(2)}) async-start(), calls=%async_computation.6 | async-start | bytes 5898240 | tf_op jit(solution)/shard_map/all_gather | solution.py:52
  367.1 1.3 copy-start
  389.4 69.7 %all-to-all-start.3 = ((bf16[2,2,262144]{2,1,0:T(2,128)(2,1)}), bf16[2,2,262144]{2,1,0:T(2,128)(2,1)S(1)}, u32[]{:S(2)}, u32[]{:S(2)}) async-start(bf16[2,2,262144]{2,1,0:T(2,128)(2,1)} %reshape.227), calls=%async_computation.3 | async-start | bytes 4194304 | tf_op jit(solution)/shard_map/all_to_all | solution.py:23
  393.4 4.2 copy-start.1
  393.4 4.2 copy-start.6
  459.1 4.9 copy-start.5
  459.1 93.3 %all-to-all-start.5 = ((bf16[8,2,122880]{2,1,0:T(2,128)(2,1)}), bf16[8,2,122880]{2,1,0:T(2,128)(2,1)}, u32[]{:S(2)}, u32[]{:S(2)}) async-start(bf16[8,2,122880]{2,1,0:T(2,128)(2,1)} %reshape.225), calls=%async_computation.5 | async-start | bytes 7864320 | tf_op jit(solution)/shard_map/all_to_all | solution.py:61
  581.8 7.9 %copy-start.3 = (bf16[8,256,512]{2,1,0:T(8,128)(2,1)S(1)}, bf16[8,256,512]{2,1,0:T(8,128)(2,1)}, u32[]{:S(2)}) copy-start(bf16[8,256,512]{2,1,0:T(8,128)(2,1)} %copy-done.2) | copy-start | bytes 6291460
Sparse Core Ops, SparseCore 0:
  313.0 52.6 all-gather.2
where the time goes:
time: 605 us; the launch traced here: 601 us
  blocking collectives  230 us (38%)
  local copies, waits for them, and re-layouts  125 us (21%)
  waiting for transfers between devices  122 us (20%)
  other arithmetic  62.2 us (10%)
  matrix products  27.7 us (5%)
  starting transfers between devices  19.8 us (3%)
  between operations  14.5 us (2%)
    all_to_all x1, blocking collectives, shards(): lax.all_to_all(outbox.reshape(experts, capacity, width), 'fs', split_axis...  178 us
    all_to_all x1, waiting for transfers between devices, shards(): back = lax.all_to_all(summed, 'fs', split_axis=1, concat_axis=0, tiled=True)  75.6 us
    all_to_all x1, blocking collectives, shards(): lax.all_to_all(down_cast, 'fs', split_axis=0, concat_axis=1, tiled=True)  51.6 us
    unnamed x26, local copies, waits for them, and re-layouts  41.9 us
    all_to_all x1, waiting for transfers between devices, shards(): lax.all_to_all(up_cast, 'fs', split_axis=0, concat_axis=1, tiled=True)  39.5 us
    unnamed x3, other arithmetic  37.4 us
    scatter x1, local copies, waits for them, and re-layouts, shards(): jnp.zeros((experts * capacity, width), jnp.bfloat16).at[target]  33.3 us
    convert_element_type x1, local copies, waits for them, and re-layouts, shards(): summed = total.astype(jnp.bfloat16)  27 us
  transfers between devices with their start and end apart: 5, of which 3 were waited for; matrix products, arithmetic and copies ran while one was open for 26% of the time, Pallas kernels for 0%

commit v1 on v0

v1 whole, which is shorter than its diff:
```python
import jax
import jax.numpy as jnp
from jax import lax
from jax.sharding import PartitionSpec as P

LIMIT = 7.0
ALPHA = 1.702
EPS = 1e-06


def shards(prompt, routes, route_weight, norm_gain, gate_train, up_train, down_train):
    tp = lax.axis_size("tp")
    experts = gate_train.shape[0]
    tok_rows, width = prompt.shape
    values = prompt.astype(jnp.float32)
    normed = (values * lax.rsqrt(jnp.mean(values * values, axis=-1, keepdims=True) + EPS)).astype(
        jnp.bfloat16
    )
    lanes = jnp.arange(experts, dtype=jnp.int32)
    scale = jnp.sum(
        jnp.where(routes[:, :, None] == lanes[None, None, :], route_weight[:, :, None], 0.0), axis=1
    )
    scale = lax.all_to_all(scale.T, "fs", split_axis=0, concat_axis=0, tiled=True)
    scale = scale.reshape(-1, 1)
    tokens = lax.all_gather(normed, "fs", axis=0, tiled=True)

    gain = norm_gain[None, :, None]
    gate_mine = lax.all_to_all(
        (gain * gate_train).astype(jnp.bfloat16), "fs", split_axis=0, concat_axis=0, tiled=True
    ).reshape(width, -1)
    up_mine = lax.all_to_all(
        (gain * up_train).astype(jnp.bfloat16), "fs", split_axis=0, concat_axis=0, tiled=True
    ).reshape(width, -1)
    down_rows = lax.all_to_all(
        down_train.astype(jnp.bfloat16), "fs", split_axis=0, concat_axis=0, tiled=True
    )
    down_rows = down_rows.reshape(-1, down_rows.shape[2])
    cols = down_rows.shape[1]
    own = gate_mine.shape[1]
    down_mine = lax.all_to_all(down_rows, "tp", split_axis=0, concat_axis=0, tiled=True)
    down_mine = down_mine.reshape(tp, own, cols).transpose(1, 0, 2).reshape(own, tp * cols)

    gate_pre = jnp.minimum(
        jnp.dot(tokens, gate_mine, preferred_element_type=jnp.float32), LIMIT
    )
    up_pre = jnp.clip(
        jnp.dot(tokens, up_mine, preferred_element_type=jnp.float32), -LIMIT, LIMIT
    )
    hidden = ((up_pre + 1.0) * gate_pre * jax.nn.sigmoid(ALPHA * gate_pre)).astype(jnp.bfloat16)
    pieces = lax.all_gather(hidden, "tp", axis=0, tiled=True)
    total = jnp.zeros((hidden.shape[0], cols), jnp.float32)
    for index in range(tp):
        total = total + jnp.dot(
            pieces[index * hidden.shape[0] : (index + 1) * hidden.shape[0]],
            down_rows[index * own : (index + 1) * own],
            preferred_element_type=jnp.float32,
        )
    weighted = (total * scale).astype(jnp.bfloat16)
    mixed = lax.psum_scatter(weighted, "fs", scatter_dimension=0, tiled=True)
    return (gate_mine[None], up_mine[None], down_mine[None], mixed)


def solution(mesh):
    return jax.shard_map(
        shards,
        mesh=mesh,
        in_specs=(
            P(("grp", "fs"), None),
            P(("grp", "fs"), None),
            P(("grp", "fs"), None),
            P("fs"),
            P(None, "fs", "tp"),
            P(None, "fs", "tp"),
            P(None, "fs", "tp"),
        ),
        out_specs=(
            P(("grp", "fs"), None, "tp"),
            P(("grp", "fs"), None, "tp"),
            P(("grp", "fs"), "tp", None),
            P(("grp", "fs"), "tp"),
        ),
        check_vma=False,
    )
```

time: 605 us -> 430 us (0.71)
  blocking collectives: 230 us -> 112 us
  local copies, waits for them, and re-layouts: 125 us -> 15.6 us
  waiting for transfers between devices: 122 us -> 208 us
  other arithmetic: 62.2 us -> 14.7 us
  matrix products: 27.7 us -> 48.9 us
    all_to_all x2 -> x1, blocking collectives: 230 us -> 112 us  [shards(): lax.all_to_all((gain * gate_train).astype(jnp.bfloat16), 'fs', split_axis...]
    all_gather x1 -> x2, waiting for transfers between devices: 0.02 us -> 102 us  [the longest x1 87 us: shards(): tokens = lax.all_gather(normed, 'fs', axis=0, tiled=True)]
    all_to_all x4, waiting for transfers between devices: 122 us -> 73.4 us  [the longest x1 48.4 us: shards(): lax.all_to_all(down_train.astype(jnp.bfloat16), 'fs', split_axis=0, conca...]
    unnamed x3 -> x0, other arithmetic: 37.4 us -> none
    unnamed x26 -> x9, local copies, waits for them, and re-layouts: 41.9 us -> 8.32 us
    scatter x1 -> x0, local copies, waits for them, and re-layouts: 33.3 us -> none  [shards(): jnp.zeros((experts * capacity, width), jnp.bfloat16).at[target]]
    reduce_scatter x0 -> x1, waiting for transfers between devices: none -> 32.1 us  [shards(): mixed = lax.psum_scatter(weighted, 'fs', scatter_dimension=0, tiled=True)]
    convert_element_type x2 -> x0, local copies, waits for them, and re-layouts: 31.3 us -> none  [the longest x1 27 us: shards(): summed = total.astype(jnp.bfloat16)]
  transfers between devices with their start and end apart: 5 -> 7, of which waited for: 3 -> 5; matrix products, arithmetic and copies ran while one was open for 26% -> 10% of each run, Pallas kernels for 0% -> 0%
where the time goes in v1:
time: 430 us; the launch traced here: 429 us
  waiting for transfers between devices  208 us (48%)
  blocking collectives  112 us (26%)
  matrix products  48.9 us (11%)
  starting transfers between devices  17.2 us (4%)
  local copies, waits for them, and re-layouts  15.6 us (4%)
  other arithmetic  14.7 us (3%)
  between operations  13.8 us (3%)
    all_to_all x1, blocking collectives, shards(): lax.all_to_all((gain * gate_train).astype(jnp.bfloat16), 'fs', split_axis...  112 us
    all_gather x1, waiting for transfers between devices, shards(): tokens = lax.all_gather(normed, 'fs', axis=0, tiled=True)  87 us
    all_to_all x1, waiting for transfers between devices, shards(): lax.all_to_all(down_train.astype(jnp.bfloat16), 'fs', split_axis=0, conca...  48.4 us
    reduce_scatter x1, waiting for transfers between devices, shards(): mixed = lax.psum_scatter(weighted, 'fs', scatter_dimension=0, tiled=True)  32.1 us
    all_to_all x1, waiting for transfers between devices, shards(): lax.all_to_all(down_rows, 'tp', split_axis=0, concat_axis=0, tiled=True)  25 us
    dot_general x2, matrix products, shards(): jnp.dot(pieces[index * hidden.shape[0]:(index + 1) * hidden.shape[0]], do...  21.8 us
    dot_general x1, matrix products, shards(): jnp.dot(tokens, up_mine, preferred_element_type=jnp.float32)  15.8 us
    all_gather x1, waiting for transfers between devices, shards(): pieces = lax.all_gather(hidden, 'tp', axis=0, tiled=True)  15 us
  transfers between devices with their start and end apart: 7, of which 5 were waited for; matrix products, arithmetic and copies ran while one was open for 10% of the time, Pallas kernels for 0%

profile of v1, /device:TPU:0, one launch (start us, length us, event | category | flops | bytes accessed | tf_op | source)
XLA Modules:
  0.0 429.3 jit_solution(14613814790445612276)
XLA Ops:
  7.2 0.0 copy-start.2
  7.2 0.0 all-gather.3.cloned.1.call-start
  7.2 1.8 fusion
  9.0 2.9 fusion.1
  11.9 0.0 all-gather.3.cloned.1.call-update
  11.9 0.0 copy-done.2
  11.9 6.1 %multiply_convert_fusion.2 = (bf16[8,256,512]{2,1,0:T(8,128)(2,1)}, bf16[8,256,512]{2,1,0:T(8,128)(2,1)S(1)}) fusion(f32[8,256,512]{2,1,0:T(8,128)} %param.12, f32[256]{0:T(256)S(1)} %copy-done.2, f32[8,256,512]{2,1,0:T(8,128)} %param.11), kind=kLoop, calls=%fused_computation.2 | loop fusion | flops 4194304 | bytes 12583936 | tf_op jit(solution)/shard_map/convert_element_type | solution.py:32
  18.1 111.5 %all_to_all.33 = bf16[8,256,512]{2,1,0:T(8,128)(2,1)S(1)} all-to-all(bf16[8,256,512]{2,1,0:T(8,128)(2,1)S(1)} %get-tuple-element.15), channel_id=1, replica_groups=mesh['grp'=2,'fs'=8,'tp'=2] {'fs'}, dimensions={0} | all-to-all | bytes 4194304 | tf_op jit(solution)/shard_map/all_to_all | solution.py:28
  129.6 4.3 %all-to-all-start.1 = ((bf16[8,256,512]{2,1,0:T(8,128)(2,1)}), bf16[8,256,512]{2,1,0:T(8,128)(2,1)}, u32[]{:S(2)}, u32[]{:S(2)}) async-start(bf16[8,256,512]{2,1,0:T(8,128)(2,1)} %get-tuple-element.14), calls=%async_computation.1 | async-start | bytes 4194304 | tf_op jit(solution)/shard_map/all_to_all | solution.py:31
  133.9 0.0 all-gather.5.cloned.1.call-start
  134.0 87.0 %all-gather.3.cloned.1.call-done = bf16[3072,2048]{1,0:T(8,128)(2,1)} async-done(((bf16[384,2048]{1,0:T(8,128)(2,1)}), bf16[3072,2048]{1,0:T(8,128)(2,1)}) %all-gather.3.cloned.1.call-update) | async-done | bytes 12582928 | tf_op jit(solution)/shard_map/all_gather | solution.py:25
  221.0 11.4 %fusion.6 = f32[3072,512]{1,0:T(8,128)} fusion(bf16[3072,2048]{1,0:T(8,128)(2,1)} %all-gather.3.cloned.1.call-done, bf16[2048,512]{1,0:T(8,128)(2,1)S(1)} %bitcast.20), kind=kOutput, calls=%fused_computation.15 | convolution fusion | flops 6442450944 | bytes 20971520 | tf_op jit(solution)/shard_map/dot_general | solution.py:44
  232.4 0.0 all-to-all-done.1
  232.4 15.8 %multiply_convert_fusion.1 = bf16[3072,512]{1,0:T(8,128)(2,1)} fusion(f32[3072,512]{1,0:T(8,128)} %fusion.6, bf16[3072,2048]{1,0:T(8,128)(2,1)} %all-gather.3.cloned.1.call-done, bf16[2048,512]{1,0:T(8,128)(2,1)} %bitcast.5), kind=kOutput, calls=%fused_computation.1 | convolution fusion | flops 6458179584 | bytes 24117248 | tf_op jit(solution)/shard_map/dot_general | solution.py:47
  248.1 0.0 all-gather.5.cloned.1.call-update
  248.1 0.0 copy-start
  248.1 0.0 copy-start.1
  248.2 3.8 convert_element_type.23
  252.0 4.4 %all-to-all-start.2 = ((bf16[8,128,1024]{2,1,0:T(8,128)(2,1)}), bf16[8,128,1024]{2,1,0:T(8,128)(2,1)}, u32[]{:S(2)}, u32[]{:S(2)}) async-start(bf16[8,128,1024]{2,1,0:T(8,128)(2,1)} %convert_element_type.23), calls=%async_computation.2 | async-start | bytes 4194304 | tf_op jit(solution)/shard_map/all_to_all | solution.py:34
  256.4 0.0 copy-done
  256.4 0.0 copy-done.1
  256.4 0.6 copy.24
  257.1 48.4 %all-to-all-done.2 = bf16[8,128,1024]{2,1,0:T(8,128)(2,1)} async-done(((bf16[8,128,1024]{2,1,0:T(8,128)(2,1)}), bf16[8,128,1024]{2,1,0:T(8,128)(2,1)}, u32[]{:S(2)}, u32[]{:S(2)}) %all-to-all-start.2) | async-done | bytes 2097184 | tf_op jit(solution)/shard_map/all_to_all | solution.py:34
  305.4 3.3 all-to-all-start.4
  308.8 0.2 reduce-scatter.2.cloned.1.call-start
  309.0 2.8 fusion.5
  311.8 15.0 %all-gather.5.cloned.1.call-done = bf16[6144,512]{1,0:T(8,128)(2,1)} async-done(((bf16[3072,512]{1,0:T(8,128)(2,1)}), bf16[6144,512]{1,0:T(8,128)(2,1)}) %all-gather.5.cloned.1.call-update) | async-done | bytes 6291472 | tf_op jit(solution)/shard_map/all_gather | solution.py:50
  326.8 10.1 %fusion.3 = f32[3072,1024]{1,0:T(8,128)} fusion(bf16[512,1024]{1,0:T(8,128)(2,1)} %bitcast.24, bf16[6144,512]{1,0:T(8,128)(2,1)} %all-gather.5.cloned.1.call-done), kind=kOutput, calls=%fused_computation.9 | convolution fusion | flops 3221225472 | bytes 16777216 | tf_op jit(solution)/shard_map/dot_general | solution.py:53
  336.9 0.0 all-to-all-done.4
  336.9 11.6 %multiply_convert_fusion = bf16[3072,1024]{1,0:T(8,128)(2,1)} fusion(f32[3072,1024]{1,0:T(8,128)} %fusion.3, f32[3072]{0:T(1024)S(1)} %bitcast.26, bf16[512,1024]{1,0:T(8,128)(2,1)S(1)} %bitcast.23, bf16[6144,512]{1,0:T(8,128)(2,1)} %all-gather.5.cloned.1.call-done), kind=kOutput, calls=%fused_computation | convolution fusion | flops 3230662656 | bytes 23080960 | tf_op jit(solution)/shard_map/dot_general | solution.py:53
  348.5 0.0 reduce-scatter.2.cloned.1.call-update
  348.6 4.8 %all-to-all-start.3 = ((bf16[2,512,1024]{2,1,0:T(8,128)(2,1)}), bf16[2,512,1024]{2,1,0:T(8,128)(2,1)}, u32[]{:S(2)}, u32[]{:S(2)}) async-start(bf16[2,512,1024]{2,1,0:T(8,128)(2,1)} %bitcast.2), calls=%async_computation.3 | async-start | bytes 4194304 | tf_op jit(solution)/shard_map/all_to_all | solution.py:40
  353.4 25.0 %all-to-all-done.3 = bf16[2,512,1024]{2,1,0:T(8,128)(2,1)} async-done(((bf16[2,512,1024]{2,1,0:T(8,128)(2,1)}), bf16[2,512,1024]{2,1,0:T(8,128)(2,1)}, u32[]{:S(2)}, u32[]{:S(2)}) %all-to-all-start.3) | async-done | bytes 2097184 | tf_op jit(solution)/shard_map/all_to_all | solution.py:40
  378.4 4.0 copy.23
  382.4 3.9 copy.25
  386.3 32.1 %reduce-scatter.2.cloned.1.call-done = bf16[384,1024]{1,0:T(8,128)(2,1)} async-done(((bf16[3072,1024]{1,0:T(8,128)(2,1)}), bf16[384,1024]{1,0:T(8,128)(2,1)}) %reduce-scatter.2.cloned.1.call-update) | async-done | bytes 786448 | tf_op jit(solution)/shard_map/reduce_scatter | solution.py:59
  418.4 1.3 copy.28
  419.8 3.0 copy.29
  (2 shorter events, 0.0 us)
Async XLA Ops:
  7.2 4.8 %copy-start.2 = (f32[256]{0:T(256)S(1)}, f32[256]{0:T(256)}, u32[]{:S(2)}) copy-start(f32[256]{0:T(256)} %param.10) | copy-start | bytes 3076
  7.2 213.8 %all-gather.3.cloned.1.call-start = ((), (), s32[]{:S(2)}) async-start(), calls=%async_computation.6 | async-start | bytes 14155776 | tf_op jit(solution)/shard_map/all_gather | solution.py:25
  129.6 102.8 %all-to-all-start.1 = ((bf16[8,256,512]{2,1,0:T(8,128)(2,1)}), bf16[8,256,512]{2,1,0:T(8,128)(2,1)}, u32[]{:S(2)}, u32[]{:S(2)}) async-start(bf16[8,256,512]{2,1,0:T(8,128)(2,1)} %get-tuple-element.14), calls=%async_computation.1 | async-start | bytes 4194304 | tf_op jit(solution)/shard_map/all_to_all | solution.py:31
  133.9 192.8 %all-gather.5.cloned.1.call-start = ((), (), s32[]{:S(2)}) async-start(), calls=%async_computation.7 | async-start | bytes 9437184 | tf_op jit(solution)/shard_map/all_gather | solution.py:50
  248.1 8.3 %copy-start = (f32[384,4]{0,1:T(4,128)S(1)}, f32[384,4]{0,1:T(4,128)}, u32[]{:S(2)}) copy-start(f32[384,4]{0,1:T(4,128)} %param.9) | copy-start | bytes 18436
  248.1 8.3 %copy-start.1 = (s32[384,4]{0,1:T(4,128)S(1)}, s32[384,4]{0,1:T(4,128)}, u32[]{:S(2)}) copy-start(s32[384,4]{0,1:T(4,128)} %param.8) | copy-start | bytes 18436
  252.0 53.4 %all-to-all-start.2 = ((bf16[8,128,1024]{2,1,0:T(8,128)(2,1)}), bf16[8,128,1024]{2,1,0:T(8,128)(2,1)}, u32[]{:S(2)}, u32[]{:S(2)}) async-start(bf16[8,128,1024]{2,1,0:T(8,128)(2,1)} %convert_element_type.23), calls=%async_computation.2 | async-start | bytes 4194304 | tf_op jit(solution)/shard_map/all_to_all | solution.py:34
  305.4 31.5 %all-to-all-start.4 = ((f32[8,1,384]{2,1,0:T(1,128)}), f32[8,1,384]{2,1,0:T(1,128)S(1)}, u32[]{:S(2)}, u32[]{:S(2)}) async-start(f32[8,1,384]{2,1,0:T(1,128)} %copy.24), calls=%async_computation.4 | async-start | bytes 24576 | tf_op jit(solution)/shard_map/all_to_all | solution.py:23
  308.8 109.7 %reduce-scatter.2.cloned.1.call-start = ((), (), s32[]{:S(2)}) async-start(), calls=%async_computation.8 | async-start | bytes 7077888 | tf_op jit(solution)/shard_map/reduce_scatter | solution.py:59
  348.6 29.9 %all-to-all-start.3 = ((bf16[2,512,1024]{2,1,0:T(8,128)(2,1)}), bf16[2,512,1024]{2,1,0:T(8,128)(2,1)}, u32[]{:S(2)}, u32[]{:S(2)}) async-start(bf16[2,512,1024]{2,1,0:T(8,128)(2,1)} %bitcast.2), calls=%async_computation.3 | async-start | bytes 4194304 | tf_op jit(solution)/shard_map/all_to_all | solution.py:40
Sparse Core Ops, SparseCore 0:
  12.0 208.8 all-gather.2
  248.3 78.4 all-gather.4
  348.7 69.7 reduce-scatter.1

commit v2 on v1

v2 whole, which is shorter than its diff:
```python
import functools

import jax
import jax.numpy as jnp
from jax import lax
from jax.experimental import pallas as pl
from jax.experimental.pallas import tpu as pltpu
from jax.sharding import PartitionSpec as P

LIMIT = 7.0
ALPHA = 1.702
EPS = 1e-06
MESH = pl.DeviceIdType.MESH


def exchange(
    sizes,
    tok_in,
    gate_in,
    up_in,
    down_in,
    tok,
    gate,
    up,
    down,
    recv_w,
    send_w,
    recv_t,
    send_up,
    send_dn,
    send_pt,
    local,
):
    G, F, T = sizes
    g, f, t = lax.axis_index("grp"), lax.axis_index("fs"), lax.axis_index("tp")
    barrier = pltpu.get_barrier_semaphore()
    for axis, here, count in (("fs", f, F), ("grp", g, G), ("tp", t, T)):
        for s in range(1, count):
            pl.semaphore_signal(
                barrier, inc=1, device_id={axis: lax.rem(here + s, count)}, device_id_type=MESH
            )
    pl.semaphore_wait(barrier, F + G + T - 3)

    def remote(src, dst, send, recv, **where):
        return pltpu.make_async_remote_copy(
            src_ref=src, dst_ref=dst, send_sem=send, recv_sem=recv, device_id=where,
            device_id_type=MESH,
        )

    mats = ((gate_in, gate), (up_in, up), (down_in, down))

    def rows_of(m, src, gg, tt):
        block = mats[m][0].shape[1]
        piece = block // G
        start = (tt * F + src) * block + gg * piece
        return mats[m][1].at[pl.ds(pl.multiple_of(start, piece), piece)]

    def sent_piece(m, expert):
        piece = mats[m][0].shape[1] // G
        return mats[m][0].at[expert, pl.ds(pl.multiple_of(g * piece, piece), piece)]

    def wait_piece(m, src, gg, tt):
        ref = rows_of(m, src, gg, tt)
        remote(ref, ref, send_w.at[m], recv_w.at[m, src, gg, tt], fs=lax.rem(f + 1, F)).wait_recv()

    def pass_on(m, src, gg, tt, **where):
        ref = rows_of(m, src, gg, tt)
        remote(ref, ref, send_w.at[m], recv_w.at[m, src, gg, tt], **where).start()

    rows = tok_in.shape[0]

    def block_of(src):
        return tok.at[pl.ds(pl.multiple_of(src * rows, rows), rows)]

    Z = F // 2
    z, core = f // 2, lax.rem(f, 2)
    partner = f + 1 - 2 * core

    own = [pltpu.make_async_copy(tok_in, block_of(f), local.at[3])]
    for m in range(3):
        own.append(pltpu.make_async_copy(sent_piece(m, f), rows_of(m, f, g, t), local.at[m]))
    for copy in own:
        copy.start()

    for m in range(3):

        @pl.loop(1, F)
        def _(s, m=m):
            to = lax.rem(f + s, F)
            remote(
                sent_piece(m, to), rows_of(m, f, g, t), send_w.at[m], recv_w.at[m, f, g, t], fs=to
            ).start()

    def tok_copy(src_ref, src, kind):
        sems, to = ((send_up, f + 2), (send_dn, f - 2), (send_pt, partner))[kind]
        return remote(src_ref, block_of(src), sems.at[src], recv_t.at[src], fs=to)

    @pl.when(z < Z - 1)
    def _():
        tok_copy(tok_in, f, 0).start()

    @pl.when(z > 0)
    def _():
        tok_copy(tok_in, f, 1).start()

    tok_copy(tok_in, f, 2).start()

    def first(m, src):
        for dg in range(1, G):
            pass_on(m, src, g, t, grp=lax.rem(g + dg, G))
        for dt in range(1, T):
            pass_on(m, src, g, t, tp=lax.rem(t + dt, T))

    def phase1(m):
        own[m + 1].wait()
        first(m, f)

        @pl.loop(1, F)
        def _(s):
            src = lax.rem(f - s + F, F)
            wait_piece(m, src, g, t)
            first(m, src)

    def phase2(m):
        @pl.loop(0, F)
        def _(s):
            src = lax.rem(f - s + F, F)
            even = lax.rem(src, 2) == 0
            for dg in range(1, G):
                gg = lax.rem(g + dg, G)
                wait_piece(m, src, gg, t)

                @pl.when(even)
                def _():
                    for dt in range(1, T):
                        pass_on(m, src, gg, t, tp=lax.rem(t + dt, T))

            for dt in range(1, T):
                tt = lax.rem(t + dt, T)
                wait_piece(m, src, g, tt)

                @pl.when(jnp.logical_not(even))
                def _():
                    for dg in range(1, G):
                        pass_on(m, src, g, tt, grp=lax.rem(g + dg, G))

    def chain(low, high):
        @pl.loop(low, high)
        def _(d):
            @pl.when(z >= d)
            def _():
                src = f - 2 * d
                tok_copy(block_of(src), src, 2).wait_recv()

                @pl.when(z < Z - 1)
                def _():
                    tok_copy(block_of(src), src, 0).start()

                tok_copy(block_of(src), src, 2).start()

            @pl.when(z + d < Z)
            def _():
                src = f + 2 * d
                tok_copy(block_of(src), src, 2).wait_recv()

                @pl.when(z > 0)
                def _():
                    tok_copy(block_of(src), src, 1).start()

                tok_copy(block_of(src), src, 2).start()

    phase1(0)
    phase1(1)
    phase2(0)
    phase1(2)
    chain(1, 2)
    phase2(1)
    chain(2, 3)
    phase2(2)
    chain(3, Z)

    for m in range(3):

        @pl.loop(0, F)
        def _(src, m=m):
            for dg in range(1, G):
                for dt in range(1, T):
                    wait_piece(m, src, lax.rem(g + dg, G), lax.rem(t + dt, T))

        out = mats[m][1]
        sent = out.at[pl.ds(0, out.shape[0] - mats[m][0].shape[1] // G)]
        remote(sent, sent, send_w.at[m], recv_w.at[m, 0, 0, 0], fs=lax.rem(f + 1, F)).wait_send()

    own[0].wait()

    @pl.loop(0, Z)
    def _(zz):
        src = 2 * zz + core
        other = 2 * zz + 1 - core
        tok_copy(block_of(other), other, 2).wait_recv()
        tok_copy(block_of(src), src, 2).wait_send()

        @pl.when(jnp.logical_and(zz <= z, z < Z - 1))
        def _():
            tok_copy(block_of(src), src, 0).wait_send()

        @pl.when(jnp.logical_and(zz >= z, z > 0))
        def _():
            tok_copy(block_of(src), src, 1).wait_send()


def gathered(mesh, tok_in, gate_in, up_in, down_in):
    G, F, T = (mesh.shape[name] for name in ("grp", "fs", "tp"))
    full = [
        jax.ShapeDtypeStruct((T * F * w.shape[1], w.shape[2]), w.dtype)
        for w in (gate_in, up_in, down_in)
    ]
    return pl.pallas_call(
        functools.partial(exchange, (G, F, T)),
        out_shape=[jax.ShapeDtypeStruct((F * tok_in.shape[0], tok_in.shape[1]), tok_in.dtype)]
        + full,
        in_specs=[pl.BlockSpec(memory_space=pl.ANY)] * 4,
        out_specs=[pl.BlockSpec(memory_space=pltpu.VMEM)] * 4,
        scratch_shapes=[
            pltpu.SemaphoreType.DMA((3, F, G, T)),
            pltpu.SemaphoreType.DMA((3,)),
            pltpu.SemaphoreType.DMA((F,)),
            pltpu.SemaphoreType.DMA((F,)),
            pltpu.SemaphoreType.DMA((F,)),
            pltpu.SemaphoreType.DMA((F,)),
            pltpu.SemaphoreType.DMA((4,)),
        ],
        compiler_params=pltpu.CompilerParams(
            collective_id=0, has_side_effects=True, vmem_limit_bytes=40 * 1024 * 1024
        ),
    )(tok_in, gate_in, up_in, down_in)


def shards(mesh, prompt, routes, route_weight, norm_gain, gate_train, up_train, down_train):
    T, F = mesh.shape["tp"], mesh.shape["fs"]
    t = lax.axis_index("tp")
    experts = gate_train.shape[0]
    tok_rows, width = prompt.shape
    part = tok_rows // T
    values = lax.dynamic_slice_in_dim(prompt, t * part, part, 0).astype(jnp.float32)
    normed = (values * lax.rsqrt(jnp.mean(values * values, axis=-1, keepdims=True) + EPS)).astype(
        jnp.bfloat16
    )
    lanes = jnp.arange(experts, dtype=jnp.int32)
    routes = lax.dynamic_slice_in_dim(routes, t * part, part, 0)
    route_weight = lax.dynamic_slice_in_dim(route_weight, t * part, part, 0)
    scale = jnp.sum(
        jnp.where(routes[:, :, None] == lanes[None, None, :], route_weight[:, :, None], 0.0), axis=1
    )
    scale = lax.all_to_all(scale.T, "fs", split_axis=0, concat_axis=0, tiled=True)
    scale = scale.reshape(-1, 1)

    gain = norm_gain[None, :, None]
    tokens, gate, up, down = gathered(
        mesh,
        normed,
        (gain * gate_train).astype(jnp.bfloat16),
        (gain * up_train).astype(jnp.bfloat16),
        down_train.astype(jnp.bfloat16),
    )
    gate, up, down = (w.reshape(T, w.shape[0] // T, w.shape[1]) for w in (gate, up, down))
    own = gate.shape[2]
    gate_mine = lax.dynamic_slice_in_dim(gate, t, 1, 0)
    up_mine = lax.dynamic_slice_in_dim(up, t, 1, 0)
    down_mine = lax.dynamic_slice_in_dim(down, t * own, own, 1)
    down_mine = down_mine.transpose(1, 0, 2).reshape(1, own, -1)

    hidden = []
    for i in range(T):
        gate_pre = jnp.dot(tokens, gate[i], preferred_element_type=jnp.float32)
        up_pre = jnp.dot(tokens, up[i], preferred_element_type=jnp.float32)
        gate_pre = jnp.minimum(gate_pre, LIMIT)
        up_pre = jnp.clip(up_pre, -LIMIT, LIMIT)
        hidden.append(
            ((up_pre + 1.0) * gate_pre * jax.nn.sigmoid(ALPHA * gate_pre)).astype(jnp.bfloat16)
        )
    hidden = jnp.concatenate(hidden, axis=1)
    weighted = [
        (jnp.dot(hidden, down[i], preferred_element_type=jnp.float32) * scale).astype(jnp.bfloat16)
        for i in range(T)
    ]
    weighted = jnp.concatenate(weighted, axis=1)
    summed = lax.psum_scatter(weighted, "fs", scatter_dimension=0, tiled=True)
    mixed = lax.all_to_all(summed, "tp", split_axis=1, concat_axis=0, tiled=True)
    return (gate_mine, up_mine, down_mine, mixed)


def solution(mesh):
    return jax.shard_map(
        functools.partial(shards, mesh),
        mesh=mesh,
        in_specs=(
            P(("grp", "fs"), None),
            P(("grp", "fs"), None),
            P(("grp", "fs"), None),
            P("fs"),
            P(None, "fs", "tp"),
            P(None, "fs", "tp"),
            P(None, "fs", "tp"),
        ),
        out_specs=(
            P(("grp", "fs"), None, "tp"),
            P(("grp", "fs"), None, "tp"),
            P(("grp", "fs"), "tp", None),
            P(("grp", "fs"), "tp"),
        ),
        check_vma=False,
    )
```

time: 430 us -> 299 us (0.70)
  waiting for transfers between devices: 208 us -> 71.7 us
  Pallas kernels: 0 us -> 134 us
  blocking collectives: 112 us -> 0 us
  matrix products: 48.9 us -> 29.3 us
  local copies, waits for them, and re-layouts: 15.6 us -> 29.4 us
  starting transfers between devices: 17.2 us -> 9.93 us
  other arithmetic: 14.7 us -> 10 us
    pallas_call x0 -> x1, Pallas kernels: none -> 134 us  [gathered(): pl.pallas_call(functools.partial(exchange, (G, F, T)), out_shape=[jax.Sha...]
    all_to_all x1 -> x0, blocking collectives: 112 us -> none  [shards(): lax.all_to_all((gain * gate_train).astype(jnp.bfloat16), 'fs', split_axis...]
    all_gather x2 -> x0, waiting for transfers between devices: 102 us -> none  [the longest x1 87 us: shards(): tokens = lax.all_gather(normed, 'fs', axis=0, tiled=True)]
    all_to_all x3 -> x1, waiting for transfers between devices: 73.4 us -> 0.01 us  [shards(): lax.all_to_all(summed, 'tp', split_axis=1, concat_axis=0, tiled=True)]
    unnamed x3 -> x2, waiting for transfers between devices: 0.05 us -> 71.7 us
    reduce_scatter x1 -> x0, waiting for transfers between devices: 32.1 us -> none  [shards(): mixed = lax.psum_scatter(weighted, 'fs', scatter_dimension=0, tiled=True)]
    dot_general x4 -> x6, matrix products: 48.9 us -> 29.3 us  [the longest x2 11 us: shards(): gate_pre = jnp.dot(tokens, gate[i], preferred_element_type=jnp.float32)]
    all_to_all x3 -> x1, starting transfers between devices: 13.6 us -> 3.54 us  [shards(): lax.all_to_all(summed, 'tp', split_axis=1, concat_axis=0, tiled=True)]
  transfers between devices with their start and end apart: 7 -> 3, of which waited for: 5 -> 1; matrix products, arithmetic and copies ran while one was open for 10% -> 14% of each run, Pallas kernels for 0% -> 45%
where the time goes in v2:
time: 299 us; the launch traced here: 298 us
  Pallas kernels  134 us (45%)
  waiting for transfers between devices  71.7 us (24%)
  local copies, waits for them, and re-layouts  29.4 us (10%)
  matrix products  29.3 us (10%)
  between operations  14.2 us (5%)
  other arithmetic  10 us (3%)
  starting transfers between devices  9.93 us (3%)
    pallas_call x1, Pallas kernels, gathered(): pl.pallas_call(functools.partial(exchange, (G, F, T)), out_shape=[jax.Sha...  134 us
    unnamed x2, waiting for transfers between devices  71.7 us
    unnamed x21, local copies, waits for them, and re-layouts  12.4 us
    dot_general x2, matrix products, shards(): gate_pre = jnp.dot(tokens, gate[i], preferred_element_type=jnp.float32)  11 us
    dot_general x2, matrix products, shards(): jnp.dot(hidden, down[i], preferred_element_type=jnp.float32) * scale  9.46 us
    dot_general x2, matrix products, shards(): up_pre = jnp.dot(tokens, up[i], preferred_element_type=jnp.float32)  8.87 us
    all_to_all x1, starting transfers between devices, shards(): lax.all_to_all(scale.T, 'fs', split_axis=0, concat_axis=0, tiled=True)  6.35 us
  transfers between devices with their start and end apart: 3, of which 1 were waited for; matrix products, arithmetic and copies ran while one was open for 14% of the time, Pallas kernels for 45%

profile of v2, /device:TPU:0, one launch (start us, length us, event | category | flops | bytes accessed | tf_op | source)
XLA Modules:
  0.0 298.4 jit_solution(11200043945887929206)
XLA Ops:
  7.2 0.0 copy-start
  7.2 0.7 copy-done
  7.9 0.1 constant_dynamic-slice_fusion
  7.9 0.8 constant_dynamic-slice_fusion.1
  8.7 0.6 copy.24
  9.3 6.4 %all-to-all-start = ((f32[8,1,192]{2,1,0:T(1,128)}), f32[8,1,192]{2,1,0:T(1,128)S(1)}, u32[]{:S(2)}, u32[]{:S(2)}) async-start(f32[8,1,192]{2,1,0:T(1,128)} %copy.24), calls=%async_computation | async-start | bytes 16384 | tf_op jit(solution)/shard_map/all_to_all | solution.py:255
  15.7 0.0 reduce-scatter.4.cloned.1.call-start
  15.7 0.0 copy-start.4
  15.7 1.5 fusion.14
  17.3 1.3 fusion.15.tok_in
  18.6 0.0 copy-start.3
  18.6 0.0 copy-start.7
  18.6 2.7 convert_element_type.31.down_in
  21.3 0.0 copy-done.4
  21.3 0.7 copy-done.3
  22.1 0.0 copy-done.7
  22.1 1.4 multiply_convert_fusion.2
  23.5 133.9 %shard_map.102 = (bf16[1536,2048]{1,0:T(8,128)(2,1)}, bf16[4096,512]{1,0:T(8,128)(2,1)S(1)}, bf16[4096,512]{1,0:T(8,128)(2,1)}, bf16[2048,1024]{1,0:T(8,128)(2,1)}) custom-call(bf16[192,2048]{1,0:T(8,128)(2,1)S(1)} %fusion.15.tok_in, bf16[8,256,512]{2,1,0:T(8,128)(2,1)S(1)} %get-tuple-element.13.gate_in, bf16[8,256,512]{2,1,0:T(8,128)(2,1)S(1)} %get-tuple-element.12.up_in, ...), custom_call_target="tpu_custom_call" | custom-call | tf_op jit(solution)/shard_map/pallas_call | solution.py:218
  157.3 0.0 copy-start.2
  157.4 0.0 copy-start.8
  157.4 7.4 %convolution_minimum_fusion.1 = f32[1536,512]{0,1:T(8,128)S(1)} fusion(bf16[1536,2048]{1,0:T(8,128)(2,1)} %get-tuple-element.11, bf16[4096,512]{1,0:T(8,128)(2,1)S(1)} %get-tuple-element.8), kind=kOutput, calls=%fused_computation.8 | convolution fusion | flops 3222011904 | bytes 11534336 | tf_op jit(solution)/shard_map/dot_general | solution.py:275
  164.8 0.0 copy-done.2
  164.8 0.0 copy-done.8
  164.8 0.0 copy-start.6
  164.8 3.6 %convolution_minimum_fusion = f32[1536,512]{0,1:T(8,128)S(1)} fusion(bf16[1536,2048]{1,0:T(8,128)(2,1)S(1)} %copy-done.8, bf16[4096,512]{1,0:T(8,128)(2,1)S(1)} %get-tuple-element.8), kind=kOutput, calls=%fused_computation.7 | convolution fusion | flops 3222011904 | bytes 11534336 | tf_op jit(solution)/shard_map/dot_general | solution.py:275
  168.4 0.0 copy-done.6
  168.4 4.4 %fusion.7 = bf16[1536,512]{0,1:T(8,128)(2,1)S(1)} fusion(f32[1536,512]{0,1:T(8,128)S(1)} %convolution_minimum_fusion.1, bf16[1536,2048]{1,0:T(8,128)(2,1)S(1)} %copy-done.8, bf16[4096,512]{1,0:T(8,128)(2,1)S(1)} %copy-done.6), kind=kOutput, calls=%fused_computation.17 | convolution fusion | flops 3228303360 | bytes 13107200 | tf_op jit(solution)/shard_map/dot_general | solution.py:276
  172.8 4.4 %fusion.6 = bf16[1536,512]{0,1:T(8,128)(2,1)S(1)} fusion(f32[1536,512]{0,1:T(8,128)S(1)} %convolution_minimum_fusion, bf16[1536,2048]{1,0:T(8,128)(2,1)S(1)} %copy-done.8, bf16[4096,512]{1,0:T(8,128)(2,1)S(1)} %copy-done.6), kind=kOutput, calls=%fused_computation.16 | convolution fusion | flops 3228303360 | bytes 13107200 | tf_op jit(solution)/shard_map/dot_general | solution.py:276
  177.3 0.0 all-to-all-done
  177.3 0.1 mul.81
  177.4 0.0 copy-start.5
  177.4 5.7 %multiply_convert_fusion.1 = bf16[1536,1024]{0,1:T(8,128)(2,1)S(1)} fusion(f32[1536]{0:T(1024)S(1)} %mul.81, bf16[2048,1024]{1,0:T(8,128)(2,1)} %get-tuple-element.10, bf16[1536,512]{0,1:T(8,128)(2,1)S(1)} %fusion.6, bf16[1536,512]{0,1:T(8,128)(2,1)S(1)} %fusion.7), kind=kOutput, calls=%fused_computation.2 | convolution fusion | flops 3230662656 | bytes 8394752 | tf_op jit(solution)/shard_map/dot_general | solution.py:284
  183.1 0.0 copy-done.5
  183.1 3.7 %multiply_convert_fusion = bf16[1536,1024]{0,1:T(8,128)(2,1)S(1)} fusion(f32[1536]{0:T(1024)S(1)} %mul.81, bf16[2048,1024]{1,0:T(8,128)(2,1)S(1)} %copy-done.5, bf16[1536,512]{0,1:T(8,128)(2,1)S(1)} %fusion.6, bf16[1536,512]{0,1:T(8,128)(2,1)S(1)} %fusion.7), kind=kOutput, calls=%fused_computation.1 | convolution fusion | flops 3230662656 | bytes 8396800 | tf_op jit(solution)/shard_map/dot_general | solution.py:284
  186.9 3.0 %pad_maximum_fusion = bf16[1536,2048]{0,1:T(8,128)(2,1)} fusion(bf16[1536,1024]{0,1:T(8,128)(2,1)S(1)} %multiply_convert_fusion, bf16[1536,1024]{0,1:T(8,128)(2,1)S(1)} %multiply_convert_fusion.1), kind=kLoop, calls=%fused_computation | loop fusion | flops 12582912 | bytes 12582912 | tf_op jit(solution)/shard_map/concatenate | solution.py:287
  189.9 8.6 %copy.26 = bf16[1536,2048]{1,0:T(8,128)(2,1)} copy(bf16[1536,2048]{0,1:T(8,128)(2,1)} %pad_maximum_fusion) | data formatting | bytes 12582912
  198.5 0.0 reduce-scatter.4.cloned.1.call-update
  198.6 71.7 %reduce-scatter.4.cloned.1.call-done = bf16[192,2048]{1,0:T(8,128)(2,1)} async-done(((bf16[1536,2048]{1,0:T(8,128)(2,1)}), bf16[192,2048]{1,0:T(8,128)(2,1)}) %reduce-scatter.4.cloned.1.call-update) | async-done | bytes 786448
  270.2 1.4 copy.27
  271.7 1.2 copy.25
  272.9 3.5 %all-to-all-start.1 = ((bf16[192,2,1024]{2,0,1:T(8,128)(2,1)}), bf16[192,2,1024]{2,0,1:T(8,128)(2,1)S(1)}, u32[]{:S(2)}, u32[]{:S(2)}) async-start(bf16[192,2,1024]{2,0,1:T(8,128)(2,1)} %copy.25), calls=%async_computation.1 | async-start | bytes 1572864 | tf_op jit(solution)/shard_map/all_to_all | solution.py:289
  276.5 1.8 dynamic-slice_bitcast_fusion
  278.2 3.5 %copy.23 = bf16[512,2,1024]{2,1,0:T(2,128)(2,1)} copy(bf16[512,2,1024]{2,0,1:T(8,128)(2,1)S(1)} %dynamic-slice_bitcast_fusion) | data formatting | bytes 4194304 | tf_op jit(solution)/shard_map/transpose | solution.py:271
  281.7 4.5 %reshape.54 = bf16[1,512,2048]{2,1,0:T(8,128)(2,1)} reshape(bf16[512,2,1024]{2,1,0:T(2,128)(2,1)} %copy.23) | data formatting | bytes 4194304 | tf_op jit(solution)/shard_map/reshape | solution.py:271
  286.2 4.5 %constant_dynamic-slice_fusion.2 = (bf16[1,2048,512]{2,1,0:T(8,128)(2,1)}, bf16[1,2048,512]{2,1,0:T(8,128)(2,1)}) fusion(bf16[2,2048,512]{2,1,0:T(8,128)(2,1)} %bitcast.21, s32[]{:T(128)S(6)} %select_n.17, bf16[2,2048,512]{2,1,0:T(8,128)(2,1)} %bitcast.17), kind=kLoop, calls=%fused_computation.33 | loop fusion | bytes 8388612 | tf_op jit(solution)/shard_map/dynamic_slice | solution.py:269
  290.7 0.0 all-to-all-done.1
  290.7 0.9 copy.29
  291.6 0.0 copy-done.1
  (4 shorter events, 0.0 us)
Async XLA Ops:
  7.2 0.7 copy-start
  9.3 168.0 %all-to-all-start = ((f32[8,1,192]{2,1,0:T(1,128)}), f32[8,1,192]{2,1,0:T(1,128)S(1)}, u32[]{:S(2)}, u32[]{:S(2)}) async-start(f32[8,1,192]{2,1,0:T(1,128)} %copy.24), calls=%async_computation | async-start | bytes 16384 | tf_op jit(solution)/shard_map/all_to_all | solution.py:255
  15.7 254.6 %reduce-scatter.4.cloned.1.call-start = ((), (), s32[]{:S(2)}) async-start(), calls=%async_computation.3 | async-start | bytes 7077888
  15.7 5.6 %copy-start.4 = (f32[8,256,512]{2,1,0:T(8,128)S(1)}, f32[8,256,512]{2,1,0:T(8,128)}, u32[]{:S(2)}) copy-start(f32[8,256,512]{2,1,0:T(8,128)} %param.11) | copy-start | bytes 12582916
  18.6 3.5 %copy-start.3 = (f32[8,256,512]{2,1,0:T(8,128)S(1)}, f32[8,256,512]{2,1,0:T(8,128)}, u32[]{:S(2)}) copy-start(f32[8,256,512]{2,1,0:T(8,128)} %param.12) | copy-start | bytes 12582916
  18.6 3.4 %copy-start.7 = (f32[256]{0:T(256)S(1)}, f32[256]{0:T(256)}, u32[]{:S(2)}) copy-start(f32[256]{0:T(256)} %param.10) | copy-start | bytes 3076
  157.3 7.4 %copy-start.2 = (bf16[4096,512]{1,0:T(8,128)(2,1)}, bf16[4096,512]{1,0:T(8,128)(2,1)S(1)}, u32[]{:S(2)}) copy-start(bf16[4096,512]{1,0:T(8,128)(2,1)S(1)} %get-tuple-element.8) | copy-start | bytes 12582916
  157.4 7.4 %copy-start.8 = (bf16[1536,2048]{1,0:T(8,128)(2,1)S(1)}, bf16[1536,2048]{1,0:T(8,128)(2,1)}, u32[]{:S(2)}) copy-start(bf16[1536,2048]{1,0:T(8,128)(2,1)} %get-tuple-element.11) | copy-start | bytes 18874372
  164.8 3.6 %copy-start.6 = (bf16[4096,512]{1,0:T(8,128)(2,1)S(1)}, bf16[4096,512]{1,0:T(8,128)(2,1)}, u32[]{:S(2)}) copy-start(bf16[4096,512]{1,0:T(8,128)(2,1)} %get-tuple-element.9) | copy-start | bytes 12582916
  177.4 5.7 %copy-start.5 = (bf16[2048,1024]{1,0:T(8,128)(2,1)S(1)}, bf16[2048,1024]{1,0:T(8,128)(2,1)}, u32[]{:S(2)}) copy-start(bf16[2048,1024]{1,0:T(8,128)(2,1)} %get-tuple-element.10) | copy-start | bytes 12582916
  272.9 17.8 %all-to-all-start.1 = ((bf16[192,2,1024]{2,0,1:T(8,128)(2,1)}), bf16[192,2,1024]{2,0,1:T(8,128)(2,1)S(1)}, u32[]{:S(2)}, u32[]{:S(2)}) async-start(bf16[192,2,1024]{2,0,1:T(8,128)(2,1)} %copy.25), calls=%async_computation.1 | async-start | bytes 1572864 | tf_op jit(solution)/shard_map/all_to_all | solution.py:289
  286.2 5.4 %copy-start.1 = (f32[384,4]{0,1:T(4,128)S(1)}, f32[384,4]{0,1:T(4,128)}, u32[]{:S(2)}) copy-start(f32[384,4]{0,1:T(4,128)} %param.9) | copy-start | bytes 18436
Sparse Core Ops, SparseCore 0:
  198.7 71.5 reduce-scatter.3

commit v3 on v2

--- a/solution.py
+++ b/solution.py
@@ -15,10 +15,12 @@
 
 def exchange(
     sizes,
+    scale_in,
     tok_in,
     gate_in,
     up_in,
     down_in,
+    scale,
     tok,
     gate,
     up,
@@ -29,6 +31,8 @@
     send_up,
     send_dn,
     send_pt,
+    recv_s,
+    send_s,
     local,
 ):
     G, F, T = sizes
@@ -76,11 +80,21 @@
     z, core = f // 2, lax.rem(f, 2)
     partner = f + 1 - 2 * core
 
+    own_scale = pltpu.make_async_copy(scale_in.at[f], scale.at[f], local.at[4])
+    own_scale.start()
+
+    def scale_copy(to, src):
+        return remote(scale_in.at[to], scale.at[src], send_s.at[to], recv_s.at[src], fs=to)
+
     own = [pltpu.make_async_copy(tok_in, block_of(f), local.at[3])]
     for m in range(3):
         own.append(pltpu.make_async_copy(sent_piece(m, f), rows_of(m, f, g, t), local.at[m]))
     for copy in own:
         copy.start()
+
+    @pl.loop(1, F)
+    def _(s):
+        scale_copy(lax.rem(f + s, F), f).start()
 
     for m in range(3):
 
@@ -192,6 +206,13 @@
         remote(sent, sent, send_w.at[m], recv_w.at[m, 0, 0, 0], fs=lax.rem(f + 1, F)).wait_send()
 
     own[0].wait()
+    own_scale.wait()
+
+    @pl.loop(1, F)
+    def _(s):
+        to = lax.rem(f + s, F)
+        scale_copy(to, to).wait_recv()
+        scale_copy(to, f).wait_send()
 
     @pl.loop(0, Z)
     def _(zz):
@@ -209,7 +230,7 @@
             tok_copy(block_of(src), src, 1).wait_send()
 
 
-def gathered(mesh, tok_in, gate_in, up_in, down_in):
+def gathered(mesh, scale_in, tok_in, gate_in, up_in, down_in):
     G, F, T = (mesh.shape[name] for name in ("grp", "fs", "tp"))
     full = [
         jax.ShapeDtypeStruct((T * F * w.shape[1], w.shape[2]), w.dtype)
@@ -217,10 +238,11 @@
     ]
     return pl.pallas_call(
         functools.partial(exchange, (G, F, T)),
-        out_shape=[jax.ShapeDtypeStruct((F * tok_in.shape[0], tok_in.shape[1]), tok_in.dtype)]
+        out_shape=[jax.ShapeDtypeStruct(scale_in.shape, scale_in.dtype)]
+        + [jax.ShapeDtypeStruct((F * tok_in.shape[0], tok_in.shape[1]), tok_in.dtype)]
         + full,
-        in_specs=[pl.BlockSpec(memory_space=pl.ANY)] * 4,
-        out_specs=[pl.BlockSpec(memory_space=pltpu.VMEM)] * 4,
+        in_specs=[pl.BlockSpec(memory_space=pl.ANY)] * 5,
+        out_specs=[pl.BlockSpec(memory_space=pltpu.VMEM)] * 5,
         scratch_shapes=[
             pltpu.SemaphoreType.DMA((3, F, G, T)),
             pltpu.SemaphoreType.DMA((3,)),
@@ -228,16 +250,18 @@
             pltpu.SemaphoreType.DMA((F,)),
             pltpu.SemaphoreType.DMA((F,)),
             pltpu.SemaphoreType.DMA((F,)),
-            pltpu.SemaphoreType.DMA((4,)),
+            pltpu.SemaphoreType.DMA((F,)),
+            pltpu.SemaphoreType.DMA((F,)),
+            pltpu.SemaphoreType.DMA((5,)),
         ],
         compiler_params=pltpu.CompilerParams(
             collective_id=0, has_side_effects=True, vmem_limit_bytes=40 * 1024 * 1024
         ),
-    )(tok_in, gate_in, up_in, down_in)
+    )(scale_in, tok_in, gate_in, up_in, down_in)
 
 
 def shards(mesh, prompt, routes, route_weight, norm_gain, gate_train, up_train, down_train):
-    T, F = mesh.shape["tp"], mesh.shape["fs"]
+    T = mesh.shape["tp"]
     t = lax.axis_index("tp")
     experts = gate_train.shape[0]
     tok_rows, width = prompt.shape
@@ -252,17 +276,17 @@
     scale = jnp.sum(
         jnp.where(routes[:, :, None] == lanes[None, None, :], route_weight[:, :, None], 0.0), axis=1
     )
-    scale = lax.all_to_all(scale.T, "fs", split_axis=0, concat_axis=0, tiled=True)
-    scale = scale.reshape(-1, 1)
 
     gain = norm_gain[None, :, None]
-    tokens, gate, up, down = gathered(
+    scale, tokens, gate, up, down = gathered(
         mesh,
+        scale.T.reshape(experts, 1, part),
         normed,
         (gain * gate_train).astype(jnp.bfloat16),
         (gain * up_train).astype(jnp.bfloat16),
         down_train.astype(jnp.bfloat16),
     )
+    scale = scale.reshape(-1, 1)
     gate, up, down = (w.reshape(T, w.shape[0] // T, w.shape[1]) for w in (gate, up, down))
     own = gate.shape[2]
     gate_mine = lax.dynamic_slice_in_dim(gate, t, 1, 0)
@@ -284,9 +308,14 @@
         (jnp.dot(hidden, down[i], preferred_element_type=jnp.float32) * scale).astype(jnp.bfloat16)
         for i in range(T)
     ]
-    weighted = jnp.concatenate(weighted, axis=1)
-    summed = lax.psum_scatter(weighted, "fs", scatter_dimension=0, tiled=True)
-    mixed = lax.all_to_all(summed, "tp", split_axis=1, concat_axis=0, tiled=True)
+    summed = jnp.stack(
+        [lax.psum_scatter(w, "fs", scatter_dimension=0, tiled=True) for w in weighted]
+    )
+    summed, gate_mine, up_mine, down_mine = lax.optimization_barrier(
+        (summed, gate_mine, up_mine, down_mine)
+    )
+    mixed = lax.all_to_all(summed, "tp", split_axis=0, concat_axis=0, tiled=True)
+    mixed = mixed.reshape(tok_rows, -1)
     return (gate_mine, up_mine, down_mine, mixed)
 
 

time: 299 us -> 292 us (0.977)
  local copies, waits for them, and re-layouts: 29.4 us -> 17.5 us
  blocking collectives: 0 us -> 11.3 us
  matrix products: 29.3 us -> 39.6 us
  starting transfers between devices: 9.93 us -> 0.08 us
  waiting for transfers between devices: 71.7 us -> 64.8 us
    unnamed x2, waiting for transfers between devices: 71.7 us -> 0.03 us
    reduce_scatter x0 -> x2, waiting for transfers between devices: none -> 64.7 us  [shards(): lax.psum_scatter(w, 'fs', scatter_dimension=0, tiled=True)]
    all_to_all x0 -> x1, blocking collectives: none -> 11.3 us  [shards(): lax.all_to_all(summed, 'tp', split_axis=0, concat_axis=0, tiled=True)]
    all_to_all x2 -> x0, starting transfers between devices: 9.89 us -> none  [the longest x1 6.35 us: shards(): lax.all_to_all(scale.T, 'fs', split_axis=0, concat_axis=0, tiled=True)]
    unnamed x21 -> x33, local copies, waits for them, and re-layouts: 12.4 us -> 5.25 us
    dot_general x2, matrix products: 8.87 us -> 13.4 us  [shards(): up_pre = jnp.dot(tokens, up[i], preferred_element_type=jnp.float32)]
    dot_general x2, matrix products: 11 us -> 14.8 us  [shards(): gate_pre = jnp.dot(tokens, gate[i], preferred_element_type=jnp.float32)]
    concatenate x1 -> x0, other arithmetic: 3.04 us -> none  [shards(): weighted = jnp.concatenate(weighted, axis=1)]
  transfers between devices with their start and end apart: 3 -> 2, of which waited for: 1 -> 2; matrix products, arithmetic and copies ran while one was open for 14% -> 6% of each run, Pallas kernels for 45% -> 0%
where the time goes in v3:
time: 292 us; the launch traced here: 291 us
  Pallas kernels  136 us (47%)
  waiting for transfers between devices  64.8 us (22%)
  matrix products  39.6 us (14%)
  local copies, waits for them, and re-layouts  17.5 us (6%)
  between operations  14.3 us (5%)
  blocking collectives  11.3 us (4%)
  other arithmetic  8.15 us (3%)
    pallas_call x1, Pallas kernels, gathered(): pl.pallas_call(functools.partial(exchange, (G, F, T)), out_shape=[jax.Sha...  136 us
    reduce_scatter x2, waiting for transfers between devices, shards(): lax.psum_scatter(w, 'fs', scatter_dimension=0, tiled=True)  64.7 us
    dot_general x2, matrix products, shards(): gate_pre = jnp.dot(tokens, gate[i], preferred_element_type=jnp.float32)  14.8 us
    dot_general x2, matrix products, shards(): up_pre = jnp.dot(tokens, up[i], preferred_element_type=jnp.float32)  13.4 us
    dot_general x2, matrix products, shards(): jnp.dot(hidden, down[i], preferred_element_type=jnp.float32) * scale  11.4 us
    all_to_all x1, blocking collectives, shards(): lax.all_to_all(summed, 'tp', split_axis=0, concat_axis=0, tiled=True)  11.3 us
  transfers between devices with their start and end apart: 2, of which 2 were waited for; matrix products, arithmetic and copies ran while one was open for 6% of the time, Pallas kernels for 0%

profile of v3, /device:TPU:0, one launch (start us, length us, event | category | flops | bytes accessed | tf_op | source)
XLA Modules:
  0.0 291.3 jit_solution(9271367192356261891)
XLA Ops:
  7.2 0.0 copy-start
  7.2 0.0 reduce-scatter.5.cloned.1.call-start
  7.2 0.6 copy-done
  7.9 0.1 constant_dynamic-slice_fusion.2
  7.9 0.8 constant_dynamic-slice_fusion.3
  8.7 0.0 copy-start.4
  8.7 1.5 fusion.14
  10.3 1.3 fusion.15.tok_in
  11.6 0.0 copy-start.3
  11.6 0.0 copy-start.7
  11.6 2.7 convert_element_type.31.down_in
  14.3 0.0 copy-done.4
  14.3 0.7 copy-done.3
  15.1 0.0 copy-done.7
  15.1 1.4 multiply_convert_fusion.2
  16.5 135.8 %shard_map.102 = (f32[8,1,192]{2,1,0:T(1,128)S(1)}, bf16[1536,2048]{1,0:T(8,128)(2,1)}, bf16[4096,512]{1,0:T(8,128)(2,1)S(1)}, bf16[4096,512]{1,0:T(8,128)(2,1)}, bf16[2048,1024]{1,0:T(8,128)(2,1)}) custom-call(f32[8,1,192]{2,1,0:T(1,128)S(1)} %reshape.51.scale_in, bf16[192,2048]{1,0:T(8,128)(2,1)S(1)} %fusion.15.tok_in, ...), custom_call_target="tpu_custom_call" | custom-call | tf_op jit(solution)/shard_map/pallas_call | solution.py:239
  152.3 0.0 copy-start.2
  152.3 0.0 copy-start.8
  152.3 9.5 %convolution_minimum_fusion = f32[1536,512]{0,1:T(8,128)} fusion(bf16[1536,2048]{1,0:T(8,128)(2,1)} %get-tuple-element.13, bf16[4096,512]{1,0:T(8,128)(2,1)S(1)} %get-tuple-element.15), kind=kOutput, calls=%fused_computation.6 | convolution fusion | flops 3222011904 | bytes 11534336 | tf_op jit(solution)/shard_map/dot_general | solution.py:299
  161.8 0.0 copy-done.2
  161.8 5.3 %convolution_minimum_fusion.1 = f32[1536,512]{0,1:T(8,128)} fusion(bf16[1536,2048]{1,0:T(8,128)(2,1)S(1)} %copy-done.8, bf16[4096,512]{1,0:T(8,128)(2,1)S(1)} %get-tuple-element.15), kind=kOutput, calls=%fused_computation.7 | convolution fusion | flops 3222011904 | bytes 11534336 | tf_op jit(solution)/shard_map/dot_general | solution.py:299
  167.1 0.1 mul.80
  167.2 8.7 %fusion.6 = bf16[1536,512]{0,1:T(8,128)(2,1)S(1)} fusion(f32[1536,512]{0,1:T(8,128)} %convolution_minimum_fusion, bf16[1536,2048]{1,0:T(8,128)(2,1)} %get-tuple-element.13, bf16[4096,512]{1,0:T(8,128)(2,1)} %get-tuple-element.14), kind=kOutput, calls=%fused_computation.15 | convolution fusion | flops 3228303360 | bytes 13107200 | tf_op jit(solution)/shard_map/dot_general | solution.py:300
  175.9 0.0 slice-done
  175.9 0.0 copy-done.6
  175.9 0.0 slice-done.1
  175.9 0.0 copy-done.9
  175.9 0.0 copy-start.10
  175.9 4.7 %fusion.7 = bf16[1536,512]{0,1:T(8,128)(2,1)S(1)} fusion(f32[1536,512]{0,1:T(8,128)S(1)} %copy-done.9, bf16[1536,2048]{1,0:T(8,128)(2,1)S(1)} %bitcast.21, bf16[4096,512]{1,0:T(8,128)(2,1)S(1)} %copy-done.6), kind=kOutput, calls=%fused_computation.16 | convolution fusion | flops 3228303360 | bytes 13107200 | tf_op jit(solution)/shard_map/dot_general | solution.py:300
  180.7 0.0 copy-start.12
  180.7 0.0 copy-done.10
  180.7 1.1 copy-done.12
  181.8 4.9 %multiply_convert_fusion = bf16[1536,1024]{1,0:T(8,128)(2,1)} fusion(f32[1536]{0:T(1024)S(1)} %mul.80, bf16[2048,1024]{1,0:T(8,128)(2,1)S(1)} %copy-done.5, bf16[1536,512]{0,1:T(8,128)(2,1)S(1)} %fusion.6, bf16[1536,512]{0,1:T(8,128)(2,1)S(1)} %fusion.7), kind=kOutput, calls=%fused_computation | convolution fusion | flops 3230662656 | bytes 8396800 | tf_op jit(solution)/shard_map/dot_general | solution.py:308
  186.7 0.0 reduce-scatter.5.cloned.1.call-update
  186.8 0.0 reduce-scatter.3.cloned.1.call-start
  186.8 1.3 copy-done.11
  188.1 0.5 copy-done.13
  188.6 6.5 %multiply_convert_fusion.1 = bf16[1536,1024]{1,0:T(8,128)(2,1)} fusion(f32[1536]{0:T(1024)S(1)} %mul.80, bf16[2048,1024]{1,0:T(8,128)(2,1)} %get-tuple-element.16, bf16[1536,512]{0,1:T(8,128)(2,1)S(1)} %copy-done.11, bf16[1536,512]{0,1:T(8,128)(2,1)S(1)} %copy-done.13), kind=kOutput, calls=%fused_computation.1 | convolution fusion | flops 3230662656 | bytes 8394752 | tf_op jit(solution)/shard_map/dot_general | solution.py:308
  195.1 0.0 reduce-scatter.3.cloned.1.call-update
  195.1 1.8 dynamic-slice_bitcast_fusion
  196.9 2.2 copy.14
  199.1 2.8 reshape.55
  201.9 4.6 %constant_dynamic-slice_fusion = (bf16[1,2048,512]{2,1,0:T(8,128)(2,1)}, bf16[1,2048,512]{2,1,0:T(8,128)(2,1)}) fusion(bf16[2,2048,512]{2,1,0:T(8,128)(2,1)} %bitcast.16, s32[]{:T(128)S(6)} %select_n.18, bf16[2,2048,512]{2,1,0:T(8,128)(2,1)} %bitcast.13), kind=kLoop, calls=%fused_computation.31 | loop fusion | bytes 8388612 | tf_op jit(solution)/shard_map/dynamic_slice | solution.py:293
  206.4 22.8 %reduce-scatter.5.cloned.1.call-done = bf16[192,1024]{1,0:T(8,128)(2,1)} async-done(((bf16[1536,1024]{1,0:T(8,128)(2,1)}), bf16[192,1024]{1,0:T(8,128)(2,1)}) %reduce-scatter.5.cloned.1.call-update) | async-done | bytes 393232 | tf_op jit(solution)/shard_map/reduce_scatter | solution.py:312
  229.2 41.9 %reduce-scatter.3.cloned.1.call-done = bf16[192,1024]{1,0:T(8,128)(2,1)} async-done(((bf16[1536,1024]{1,0:T(8,128)(2,1)}), bf16[192,1024]{1,0:T(8,128)(2,1)}) %reduce-scatter.3.cloned.1.call-update) | async-done | bytes 393232 | tf_op jit(solution)/shard_map/reduce_scatter | solution.py:312
  271.2 1.2 pad_maximum_fusion.3
  272.4 11.3 %all_to_all.5 = bf16[2,192,1024]{2,1,0:T(8,128)(2,1)S(1)} all-to-all(bf16[2,192,1024]{2,1,0:T(8,128)(2,1)S(1)} %pad_maximum_fusion.3), channel_id=1, replica_groups=mesh['grp'=2,'fs'=8,'tp'=2] {'tp'}, dimensions={0} | all-to-all | bytes 1572864 | tf_op jit(solution)/shard_map/all_to_all | solution.py:317
  283.6 0.9 copy.16
  (16 shorter events, 0.1 us)
Async XLA Ops:
  7.2 0.7 copy-start
  7.2 222.1 %reduce-scatter.5.cloned.1.call-start = ((), (), s32[]{:S(2)}) async-start(), calls=%async_computation.4 | async-start | bytes 3538944 | tf_op jit(solution)/shard_map/reduce_scatter | solution.py:312
  8.7 5.6 %copy-start.4 = (f32[8,256,512]{2,1,0:T(8,128)S(1)}, f32[8,256,512]{2,1,0:T(8,128)}, u32[]{:S(2)}) copy-start(f32[8,256,512]{2,1,0:T(8,128)} %param.11) | copy-start | bytes 12582916
  11.6 3.5 %copy-start.3 = (f32[8,256,512]{2,1,0:T(8,128)S(1)}, f32[8,256,512]{2,1,0:T(8,128)}, u32[]{:S(2)}) copy-start(f32[8,256,512]{2,1,0:T(8,128)} %param.12) | copy-start | bytes 12582916
  11.6 3.4 %copy-start.7 = (f32[256]{0:T(256)S(1)}, f32[256]{0:T(256)}, u32[]{:S(2)}) copy-start(f32[256]{0:T(256)} %param.10) | copy-start | bytes 3076
  152.3 9.5 %copy-start.2 = (bf16[4096,512]{1,0:T(8,128)(2,1)}, bf16[4096,512]{1,0:T(8,128)(2,1)S(1)}, u32[]{:S(2)}) copy-start(bf16[4096,512]{1,0:T(8,128)(2,1)S(1)} %get-tuple-element.15) | copy-start | bytes 12582916
  152.3 9.5 %copy-start.8 = (bf16[1536,2048]{1,0:T(8,128)(2,1)S(1)}, bf16[1536,2048]{1,0:T(8,128)(2,1)}, u32[]{:S(2)}) copy-start(bf16[1536,2048]{1,0:T(8,128)(2,1)} %get-tuple-element.13) | copy-start | bytes 18874372
  161.8 14.1 %slice-start = ((s8[6291456]{0:T(1024)(128)(4,1)}), s8[2097152]{0:T(1024)(128)(4,1)S(1)}, s32[]{:S(2)}) async-start(s8[6291456]{0:T(1024)(128)(4,1)} %bitcast.20), calls=%async_computation.5 | async-start | bytes 4194304
  167.2 8.7 %copy-start.6 = (bf16[4096,512]{1,0:T(8,128)(2,1)S(1)}, bf16[4096,512]{1,0:T(8,128)(2,1)}, u32[]{:S(2)}) copy-start(bf16[4096,512]{1,0:T(8,128)(2,1)} %get-tuple-element.14) | copy-start | bytes 12582916
  167.2 8.7 %slice-start.1 = ((s8[6291456]{0:T(1024)(128)(4,1)}), s8[4194304]{0:T(1024)(128)(4,1)S(1)}, s32[]{:S(2)}) async-start(s8[6291456]{0:T(1024)(128)(4,1)} %bitcast.20), calls=%async_computation.6 | async-start | bytes 8388608
  167.2 8.7 %copy-start.9 = (f32[1536,512]{0,1:T(8,128)S(1)}, f32[1536,512]{0,1:T(8,128)}, u32[]{:S(2)}) copy-start(f32[1536,512]{0,1:T(8,128)} %convolution_minimum_fusion.1) | copy-start | bytes 9437188
  175.9 4.8 %copy-start.10 = (bf16[1536,512]{0,1:T(8,128)(2,1)}, bf16[1536,512]{0,1:T(8,128)(2,1)S(1)}, u32[]{:S(2)}) copy-start(bf16[1536,512]{0,1:T(8,128)(2,1)S(1)} %fusion.6) | copy-start | bytes 4718596
  175.9 5.9 %copy-start.5 = (bf16[2048,1024]{1,0:T(8,128)(2,1)S(1)}, bf16[2048,1024]{1,0:T(8,128)(2,1)}, u32[]{:S(2)}) copy-start(bf16[2048,1024]{1,0:T(8,128)(2,1)} %get-tuple-element.16) | copy-start | bytes 12582916
  180.7 1.1 copy-start.12
  186.7 1.4 copy-start.11
  186.7 1.9 copy-start.13
  186.8 84.4 %reduce-scatter.3.cloned.1.call-start = ((), (), s32[]{:S(2)}) async-start(), calls=%async_computation.3 | async-start | bytes 3538944 | tf_op jit(solution)/shard_map/reduce_scatter | solution.py:312
  201.9 82.6 %copy-start.1 = (f32[384,4]{0,1:T(4,128)S(1)}, f32[384,4]{0,1:T(4,128)}, u32[]{:S(2)}) copy-start(f32[384,4]{0,1:T(4,128)} %param.9) | copy-start | bytes 18436
Sparse Core Ops, SparseCore 0:
  186.9 42.3 reduce-scatter.4
  231.5 39.5 reduce-scatter.2
